TPU v7x, 32 devices: a whole 2x2x4 slice. The times are simulated.
32 devices in a mesh: fs: 16 (over z, y, x), tp: 2 (over core).
Axes of the slice: x: 2, y: 2, z: 4, core: 2. Of those that a mesh axis runs over, the one named last changes fastest.
Arguments:
- late_input: bfloat16 [2048, 2048], P('fs', 'tp'), may hold values from -6 to 6
- up_weight: bfloat16 [2048, 4096], P('tp', 'fs'), may hold values from -0.125 to 0.125
- down_weight: bfloat16 [4096, 2048], P('fs', 'tp'), may hold values from -0.09375 to 0.09375
- early_input: bfloat16 [2048, 2048], P('fs', 'tp'), may hold values from -6 to 6
- early_pre: bfloat16 [2048, 4096], P('fs'), may hold values from -6 to 6
- cotangent: bfloat16 [2048, 2048], P('fs', 'tp'), may hold values from -6 to 6
- up_sum: float32 [2048, 4096], P('tp', 'fs'), may hold values from -24 to 24
- down_sum: float32 [4096, 2048], P('fs', 'tp'), may hold values from -24 to 24
Outputs:
- late_pre: bfloat16 [2048, 4096], P('fs')
- late_out: bfloat16 [2048, 2048], P('fs', 'tp')
- input_grad: bfloat16 [2048, 2048], P('fs', 'tp')
- up_total: float32 [2048, 4096], P('tp', 'fs')
- down_total: float32 [4096, 2048], P('fs', 'tp')
All inputs are finite; a program needn't handle non-finite values.
Results may differ from a plain program's by a relative error of at most 0.025.
Values may be sent and summed in bfloat16 or wider, within the bound.
A program may use at most 128 MiB of HBM per device.

v0:
```python
import jax
import jax.numpy as jnp
from jax import lax
from jax.sharding import PartitionSpec as P


def contract_rows(left, right):
    return lax.dot_general(
        left, right, (((0,), (0,)), ((), ())), preferred_element_type=jnp.float32
    )


def contract_cols(left, right):
    return lax.dot_general(
        left, right, (((1,), (1,)), ((), ())), preferred_element_type=jnp.float32
    )


def body(late_input, up_weight, down_weight, early_input, early_pre, cotangent, up_sum, down_sum):
    up_gathered = lax.all_gather(up_weight, "fs", axis=1, tiled=True)
    down_gathered = lax.all_gather(down_weight, "fs", axis=0, tiled=True)
    pre_terms = jnp.dot(late_input, up_gathered, preferred_element_type=jnp.float32)
    pre_summed = lax.psum(pre_terms.astype(jnp.bfloat16), "tp")
    late_hidden = jnp.square(jax.nn.relu(pre_summed.astype(jnp.float32))).astype(jnp.bfloat16)
    early_float = early_pre.astype(jnp.float32)
    early_hidden = jnp.square(jax.nn.relu(early_float)).astype(jnp.bfloat16)
    late_out = jnp.dot(late_hidden, down_gathered, preferred_element_type=jnp.float32).astype(
        jnp.bfloat16
    )
    grad_terms = contract_cols(cotangent, down_gathered)
    hidden_grad = lax.psum(grad_terms.astype(jnp.bfloat16), "tp").astype(jnp.float32)
    pre_grad = (hidden_grad * 2.0 * jax.nn.relu(early_float)).astype(jnp.bfloat16)
    input_grad = contract_cols(pre_grad, up_gathered).astype(jnp.bfloat16)
    grad_local, hidden_local = (
        lax.all_to_all(pre_grad, "fs", split_axis=1, concat_axis=0, tiled=True),
        lax.all_to_all(early_hidden, "fs", split_axis=1, concat_axis=0, tiled=True),
    )
    rows = grad_local
    up_grad = contract_rows(lax.all_gather(early_input, "fs", axis=0, tiled=True), rows)
    up_total = up_sum + up_grad
    rows = hidden_local
    down_grad = contract_rows(rows, lax.all_gather(cotangent, "fs", axis=0, tiled=True))
    down_total = down_sum + down_grad
    return (pre_summed, late_out, input_grad, up_total, down_total)


def solution(mesh):
    in_specs = (
        P("fs", "tp"),
        P("tp", "fs"),
        P("fs", "tp"),
        P("fs", "tp"),
        P("fs", None),
        P("fs", "tp"),
        P("tp", "fs"),
        P("fs", "tp"),
    )
    out_specs = (P("fs", None), P("fs", "tp"), P("fs", "tp"), P("tp", "fs"), P("fs", "tp"))
    return jax.shard_map(body, mesh=mesh, in_specs=in_specs, out_specs=out_specs, check_vma=False)
```

profile of v0, /device:TPU:8, one launch (start us, length us, event | category | flops | bytes accessed | tf_op | source)
XLA Modules:
  0.0 474.2 jit_solution(18036895991787188094)
XLA Ops:
  7.2 0.0 copy-start
  7.2 0.0 all-gather.7.cloned.1.call-start
  7.2 0.7 all-gather.7.cloned.1.call-update
  7.9 0.0 all-gather.5.cloned.1.call-start
  8.0 0.7 all-gather.5.cloned.1.call-update
  8.7 0.0 all-reduce.3.cloned.1.call-start
  8.7 114.6 %all-gather.7.cloned.1.call-done = bf16[4096,1024]{1,0:T(8,128)(2,1)} async-done(((bf16[256,1024]{1,0:T(8,128)(2,1)}), bf16[4096,1024]{1,0:T(8,128)(2,1)}) %all-gather.7.cloned.1.call-update) | async-done | bytes 8388624 | tf_op jit(solution)/shard_map/all_gather | solution.py:21
  123.3 7.3 %convolution_convert_fusion = bf16[128,4096]{1,0:T(8,128)(2,1)} fusion(bf16[128,1024]{1,0:T(8,128)(2,1)} %param.13, bf16[4096,1024]{1,0:T(8,128)(2,1)} %all-gather.7.cloned.1.call-done), kind=kOutput, calls=%fused_computation | convolution fusion | flops 1074266112 | bytes 9699328 | tf_op jit(solution)/shard_map/dot_general | solution.py:14
  130.7 126.0 %all-gather.5.cloned.1.call-done = bf16[1024,4096]{1,0:T(8,128)(2,1)} async-done(((bf16[1024,256]{1,0:T(8,128)(2,1)}), bf16[1024,4096]{1,0:T(8,128)(2,1)}) %all-gather.5.cloned.1.call-update) | async-done | bytes 8388624 | tf_op jit(solution)/shard_map/all_gather | solution.py:20
  256.7 5.6 %convolution_convert_fusion.1 = bf16[128,4096]{1,0:T(8,128)(2,1)} fusion(bf16[128,1024]{1,0:T(8,128)(2,1)S(1)} %copy-done, bf16[1024,4096]{1,0:T(8,128)(2,1)} %all-gather.5.cloned.1.call-done), kind=kOutput, calls=%fused_computation.1 | convolution fusion | flops 1074266112 | bytes 9699328 | tf_op jit(solution)/shard_map/dot_general | solution.py:22
  262.3 0.0 all-reduce.3.cloned.1.call-update
  262.3 0.0 all-gather.9.cloned.1.call-start
  262.4 0.5 all-gather.9.cloned.1.call-update
  262.9 0.0 all-gather.11.cloned.1.call-start
  263.0 0.5 all-gather.11.cloned.1.call-update
  263.5 21.8 %all-reduce.3.cloned.1.call-done = (bf16[128,4096]{1,0:T(8,128)(2,1)}, bf16[128,4096]{1,0:T(8,128)(2,1)}) async-done(((bf16[128,4096]{1,0:T(8,128)(2,1)}, bf16[128,4096]{1,0:T(8,128)(2,1)}), (bf16[128,4096]{1,0:T(8,128)(2,1)}, bf16[128,4096]{1,0:T(8,128)(2,1)})) %all-reduce.3.cloned.1.call-update) | async-done | bytes 2097168 | tf_op jit(solution)/shard_map/psum | solution.py:23
  285.3 1.7 multiply_convert_fusion
  287.1 0.0 copy-start.1
  287.1 1.1 copy.24
  288.1 7.0 %all-to-all-start = ((bf16[128,16,256]{2,0,1:T(8,128)(2,1)}), bf16[128,16,256]{2,0,1:T(8,128)(2,1)}, u32[]{:S(2)}, u32[]{:S(2)}) async-start(bf16[128,16,256]{2,0,1:T(8,128)(2,1)} %bitcast.28), calls=%async_computation | async-start | bytes 2097152 | tf_op jit(solution)/shard_map/all_to_all | solution.py:35
  295.1 1.1 copy.23
  296.2 30.6 %all-to-all-done = bf16[128,16,256]{2,0,1:T(8,128)(2,1)} async-done(((bf16[128,16,256]{2,0,1:T(8,128)(2,1)}), bf16[128,16,256]{2,0,1:T(8,128)(2,1)}, u32[]{:S(2)}, u32[]{:S(2)}) %all-to-all-start) | async-done | bytes 1048608 | tf_op jit(solution)/shard_map/all_to_all | solution.py:35
  326.8 5.2 %all-to-all-start.1 = ((bf16[128,16,256]{2,0,1:T(8,128)(2,1)}), bf16[128,16,256]{2,0,1:T(8,128)(2,1)}, u32[]{:S(2)}, u32[]{:S(2)}) async-start(bf16[128,16,256]{2,0,1:T(8,128)(2,1)} %bitcast.27), calls=%async_computation.1 | async-start | bytes 2097152 | tf_op jit(solution)/shard_map/all_to_all | solution.py:36
  332.0 1.3 copy.16
  333.3 7.1 %convolution_convert_fusion.2 = bf16[128,1024]{1,0:T(8,128)(2,1)} fusion(bf16[128,4096]{1,0:T(8,128)(2,1)S(1)} %get-tuple-element.18, bf16[1024,4096]{1,0:T(8,128)(2,1)} %all-gather.5.cloned.1.call-done), kind=kOutput, calls=%fused_computation.9 | convolution fusion | flops 1073872896 | bytes 9699328 | tf_op jit(solution)/shard_map/dot_general | solution.py:14
  340.4 5.4 %convolution_convert_fusion.3 = bf16[128,1024]{1,0:T(8,128)(2,1)} fusion(bf16[4096,1024]{1,0:T(8,128)(2,1)} %all-gather.7.cloned.1.call-done, bf16[128,4096]{1,0:T(8,128)(2,1)S(1)} %copy-done.2), kind=kOutput, calls=%fused_computation.10 | convolution fusion | flops 1075970048 | bytes 9699328 | tf_op jit(solution)/shard_map/dot_general | solution.py:27
  345.8 37.0 %all-gather.9.cloned.1.call-done = bf16[2048,1024]{1,0:T(8,128)(2,1)} async-done(((bf16[128,1024]{1,0:T(8,128)(2,1)}), bf16[2048,1024]{1,0:T(8,128)(2,1)}) %all-gather.9.cloned.1.call-update) | async-done | bytes 4194320 | tf_op jit(solution)/shard_map/all_gather | solution.py:39
  382.8 3.8 fusion
  386.6 1.3 copy.18
  387.9 73.7 %all-gather.11.cloned.1.call-done = bf16[2048,1024]{1,0:T(8,128)(2,1)} async-done(((bf16[128,1024]{1,0:T(8,128)(2,1)}), bf16[2048,1024]{1,0:T(8,128)(2,1)}) %all-gather.11.cloned.1.call-update) | async-done | bytes 4194320 | tf_op jit(solution)/shard_map/all_gather | solution.py:42
  461.6 5.0 %convolution_add_fusion = f32[256,1024]{1,0:T(8,128)} fusion(f32[256,1024]{1,0:T(8,128)} %param.15, bf16[2048,256]{1,0:T(8,128)(2,1)} %bitcast.4, bf16[2048,1024]{1,0:T(8,128)(2,1)} %all-gather.11.cloned.1.call-done), kind=kOutput, calls=%fused_computation.8 | convolution fusion | flops 1074003968 | bytes 7340032 | tf_op jit(solution)/shard_map/dot_general | solution.py:8
  466.7 1.0 copy.27
  (9 shorter events, 0.0 us)
Async XLA Ops:
  7.2 249.5 %copy-start = (bf16[128,1024]{1,0:T(8,128)(2,1)S(1)}, bf16[128,1024]{1,0:T(8,128)(2,1)}, u32[]{:S(2)}) copy-start(bf16[128,1024]{1,0:T(8,128)(2,1)} %param.8) | copy-start | bytes 786436
  7.2 116.2 %all-gather.7.cloned.1.call-start = ((), (), s32[]{:S(2)}) async-start(), calls=%async_computation.3 | async-start | bytes 8912896 | tf_op jit(solution)/shard_map/all_gather | solution.py:21
  7.9 248.8 %all-gather.5.cloned.1.call-start = ((), (), s32[]{:S(2)}) async-start(), calls=%async_computation.2 | async-start | bytes 8912896 | tf_op jit(solution)/shard_map/all_gather | solution.py:20
  8.7 276.6 %all-reduce.3.cloned.1.call-start = ((), (), s32[]{:S(2)}) async-start(), calls=%async_computation.6 | async-start | bytes 4194304 | tf_op jit(solution)/shard_map/psum | solution.py:23
  130.7 154.6 %copy-start.4 = (bf16[128,4096]{1,0:T(8,128)(2,1)S(1)}, bf16[128,4096]{1,0:T(8,128)(2,1)}, u32[]{:S(2)}) copy-start(bf16[128,4096]{1,0:T(8,128)(2,1)} %param.12) | copy-start | bytes 3145732
  262.3 120.4 %all-gather.9.cloned.1.call-start = ((), (), s32[]{:S(2)}) async-start(), calls=%async_computation.4 | async-start | bytes 4456448 | tf_op jit(solution)/shard_map/all_gather | solution.py:39
  262.9 198.7 %all-gather.11.cloned.1.call-start = ((), (), s32[]{:S(2)}) async-start(), calls=%async_computation.5 | async-start | bytes 4456448 | tf_op jit(solution)/shard_map/all_gather | solution.py:42
  287.1 44.9 %copy-start.1 = (f32[1024,256]{1,0:T(8,128)S(1)}, f32[1024,256]{1,0:T(8,128)}, u32[]{:S(2)}) copy-start(f32[1024,256]{1,0:T(8,128)} %param.14) | copy-start | bytes 3145732
  288.1 38.6 %all-to-all-start = ((bf16[128,16,256]{2,0,1:T(8,128)(2,1)}), bf16[128,16,256]{2,0,1:T(8,128)(2,1)}, u32[]{:S(2)}, u32[]{:S(2)}) async-start(bf16[128,16,256]{2,0,1:T(8,128)(2,1)} %bitcast.28), calls=%async_computation | async-start | bytes 2097152 | tf_op jit(solution)/shard_map/all_to_all | solution.py:35
  326.8 134.8 %all-to-all-start.1 = ((bf16[128,16,256]{2,0,1:T(8,128)(2,1)}), bf16[128,16,256]{2,0,1:T(8,128)(2,1)}, u32[]{:S(2)}, u32[]{:S(2)}) async-start(bf16[128,16,256]{2,0,1:T(8,128)(2,1)} %bitcast.27), calls=%async_computation.1 | async-start | bytes 2097152 | tf_op jit(solution)/shard_map/all_to_all | solution.py:36
  333.3 7.1 %copy-start.2 = (bf16[128,4096]{1,0:T(8,128)(2,1)S(1)}, bf16[128,4096]{1,0:T(8,128)(2,1)}, u32[]{:S(2)}) copy-start(bf16[128,4096]{1,0:T(8,128)(2,1)} %get-tuple-element.19) | copy-start | bytes 3145732
  340.4 42.4 %copy-start.3 = (f32[1024,256]{0,1:T(8,128)S(1)}, f32[1024,256]{0,1:T(8,128)}, u32[]{:S(2)}) copy-start(f32[1024,256]{0,1:T(8,128)} %copy.16) | copy-start | bytes 3145732
Sparse Core Ops, SparseCore 0:
  10.8 112.5 all-gather.6
  126.0 130.6 all-gather.4
  262.5 22.8 all-reduce.2
  287.9 94.7 all-gather.8
  385.4 76.1 all-gather.10
where the time goes:
time: 476 us; the launch traced here: 474 us
  waiting for transfers between devices  406 us (85%)
  matrix products  34.3 us (7%)
  between operations  13.8 us (3%)
  starting transfers between devices  12.3 us (3%)
  local copies, waits for them, and re-layouts  5.76 us (1%)
    all_gather x1, waiting for transfers between devices, body(): up_gathered = lax.all_gather(up_weight, 'fs', axis=1, tiled=True)  126 us
    all_gather x1, waiting for transfers between devices, body(): down_gathered = lax.all_gather(down_weight, 'fs', axis=0, tiled=True)  115 us
    all_gather x1, waiting for transfers between devices, body(): lax.all_gather(cotangent, 'fs', axis=0, tiled=True)  73.7 us
    all_gather x1, waiting for transfers between devices, body(): lax.all_gather(early_input, 'fs', axis=0, tiled=True)  37 us
    all_to_all x1, waiting for transfers between devices, body(): lax.all_to_all(pre_grad, 'fs', split_axis=1, concat_axis=0, tiled=True)  30.6 us
    psum x1, waiting for transfers between devices, body(): pre_summed = lax.psum(pre_terms.astype(jnp.bfloat16), 'tp')  21.8 us
    dot_general x2, matrix products, contract_cols(): lax.dot_general(left, right, (((1,), (1,)), ((), ())), preferred_element_...  14.4 us
  transfers between devices with their start and end apart: 7, of which 6 were waited for; matrix products, arithmetic and copies ran while one was open for 6% of the time, Pallas kernels for 0%

commit v1 on v0

--- a/solution.py
+++ b/solution.py
@@ -1,7 +1,361 @@
 import jax
 import jax.numpy as jnp
 from jax import lax
+from jax.experimental import pallas as pl
+from jax.experimental.pallas import tpu as pltpu
 from jax.sharding import PartitionSpec as P
+
+MESH = pl.DeviceIdType.MESH
+F32 = jnp.float32
+BF16 = jnp.bfloat16
+
+
+def dot(left, right, lc, rc):
+    return lax.dot_general(left, right, (((lc,), (rc,)), ((), ())), preferred_element_type=F32)
+
+
+def square_relu(value):
+    kept = jnp.maximum(value.astype(F32), 0.0)
+    return (kept * kept).astype(BF16)
+
+
+def fused(a, late_in, up_w, down_w, early_in, early_pre, cot, up_sum, down_sum,
+          late_pre_o, late_out_o, in_grad_o, up_o, down_o,
+          cot_g, late_g, early_g, pre_g, up_g, down_g, gt_s, gt_r, pg, eh, lt_s, lt_r, lp, lh, lp_g,
+          part, ig_s, ig_u, ig_d, lo_s, lo_u, lo_d,
+          dg_s, dg_x, dg_y, dg_fx, dg_fy, ug_s, ug_x, ug_y, ug_fx, ug_fy,
+          ag_ss, ag_rs, w_ss, w_rs, e_ss, e_rs, l_ss, l_rs, t_ss, t_rs, rl_ss, rl_rs, rq_ss, rq_rs):
+    side = 4
+    half_side = side // 2
+    me = lax.axis_index("fs")
+    t = lax.axis_index("tp")
+    z = me // side
+    q = lax.rem(me, side)
+    y = q // 2
+    x = lax.rem(q, 2)
+    qx = y * 2 + (1 - x)
+    qy = (1 - y) * 2 + x
+    qd = side - 1 - q
+    xn = (z * side + qx, t)
+    yn = (z * side + qy, t)
+    pn = (me, 1 - t)
+    above = (lax.rem(me + side, a * side), t)
+    below = (lax.rem(me + (a - 1) * side, a * side), t)
+    rows = late_in.shape[0]
+    ff = up_w.shape[1]
+    width = late_in.shape[1]
+    cols = ff * side
+    step_n = width // side
+
+    barrier = pltpu.get_barrier_semaphore()
+    greet = [xn, yn, pn] + [(lax.rem(me + o * side, a * side), t) for o in range(1, a)]
+    for device in greet:
+        pl.semaphore_signal(barrier, inc=1, device_id=device, device_id_type=MESH)
+    pl.semaphore_wait(barrier, len(greet))
+
+    sent = []
+
+    def rc(src, dst, ss, rs, device):
+        return pltpu.make_async_remote_copy(
+            src_ref=src, dst_ref=dst, send_sem=ss, recv_sem=rs, device_id=device, device_id_type=MESH)
+
+    def send(src, dst, ss, rs, device, cond=None):
+        def go():
+            rc(src, dst, ss, rs, device).start()
+
+        if cond is None:
+            go()
+        else:
+            pl.when(cond)(go)
+        sent.append((cond, rc(src, dst, ss, rs, device)))
+
+    def arrive(dst, ss, rs, cond=None):
+        def go():
+            rc(dst, dst, ss, rs, pn).wait_recv()
+
+        if cond is None:
+            go()
+        else:
+            pl.when(cond)(go)
+
+    def slot(j):
+        return pl.ds(pl.multiple_of(j * rows, rows), rows)
+
+    def line_gather(which, own, buf, d):
+        for way in range(2):
+            if way == 0:
+                j, here, on, device = z - d, z >= d, (z >= d) & (z < a - 1), above
+            else:
+                j, here, on, device = z + d, z + d < a, (z + d < a) & (z > 0), below
+            j = jnp.clip(j, 0, a - 1)
+            place = buf.at[slot(j)]
+            if d > 0:
+                arrive(place, ag_ss.at[which, way, 0], ag_rs.at[which, way, d], here)
+            if d < a - 1:
+                send(own if d == 0 else place, place, ag_ss.at[which, way, d],
+                     ag_rs.at[which, way, d + 1], device, on)
+
+    def half(ref, block, h):
+        n = ref.shape[1] // 2
+        return ref.at[block, pl.ds(h * n, n)]
+
+    def half2(ref, h):
+        n = ref.shape[0] // 2
+        return ref.at[pl.ds(h * n, n)]
+
+    def square_send(which, own, buf):
+        for h in (0, 1):
+            send(half2(own, h), half(buf, q, h), w_ss.at[which, 0, h], w_rs.at[which, 0, h], xn)
+            send(half2(own, 1 - h), half(buf, q, 1 - h), w_ss.at[which, 1, 1 - h], w_rs.at[which, 1, 1 - h], yn)
+
+    def square_relay(which, buf):
+        arrive(half(buf, qx, 0), w_ss.at[which, 0, 0], w_rs.at[which, 0, 0])
+        send(half(buf, qx, 0), half(buf, qx, 0), w_ss.at[which, 1, 2], w_rs.at[which, 1, 2], yn)
+        arrive(half(buf, qy, 1), w_ss.at[which, 0, 0], w_rs.at[which, 1, 1])
+        send(half(buf, qy, 1), half(buf, qy, 1), w_ss.at[which, 0, 2], w_rs.at[which, 0, 2], xn)
+
+    def square_rest(which, buf):
+        arrive(half(buf, qx, 1), w_ss.at[which, 0, 0], w_rs.at[which, 0, 1])
+        arrive(half(buf, qy, 0), w_ss.at[which, 0, 0], w_rs.at[which, 1, 0])
+        arrive(half(buf, qd, 0), w_ss.at[which, 0, 0], w_rs.at[which, 1, 2])
+        arrive(half(buf, qd, 1), w_ss.at[which, 0, 0], w_rs.at[which, 0, 2])
+
+    def square_sum_begin(which, block, staged, first_x, first_y, fin_x, fin_y):
+        staged[qd] = block(qd).astype(BF16)
+        send(half(staged, qd, 0), first_x, rq_ss.at[which, 0], rq_rs.at[which, 0], xn)
+        send(half(staged, qd, 1), first_y, rq_ss.at[which, 1], rq_rs.at[which, 1], yn)
+        staged[qx] = block(qx).astype(BF16)
+        send(half(staged, qx, 0), half2(fin_x, 0), rq_ss.at[which, 2], rq_rs.at[which, 2], xn)
+        staged[qy] = block(qy).astype(BF16)
+        send(half(staged, qy, 1), half2(fin_y, 1), rq_ss.at[which, 3], rq_rs.at[which, 3], yn)
+
+    def square_sum_relay(which, staged, first_x, first_y, fin_x, fin_y):
+        n = staged.shape[1] // 2
+        arrive(first_x, rq_ss.at[which, 0], rq_rs.at[which, 0])
+        staged[qy, 0:n] = (staged[qy, 0:n].astype(F32) + first_x[...].astype(F32)).astype(BF16)
+        send(half(staged, qy, 0), half2(fin_y, 0), rq_ss.at[which, 4], rq_rs.at[which, 4], yn)
+        arrive(first_y, rq_ss.at[which, 0], rq_rs.at[which, 1])
+        staged[qx, n:2 * n] = (staged[qx, n:2 * n].astype(F32) + first_y[...].astype(F32)).astype(BF16)
+        send(half(staged, qx, 1), half2(fin_x, 1), rq_ss.at[which, 5], rq_rs.at[which, 5], xn)
+
+    def square_sum_end(which, fin_x, fin_y, out):
+        arrive(half2(fin_x, 0), rq_ss.at[which, 0], rq_rs.at[which, 2])
+        arrive(half2(fin_y, 1), rq_ss.at[which, 0], rq_rs.at[which, 3])
+        arrive(half2(fin_y, 0), rq_ss.at[which, 0], rq_rs.at[which, 4])
+        arrive(half2(fin_x, 1), rq_ss.at[which, 0], rq_rs.at[which, 5])
+        out[...] = out[...] + (fin_x[...].astype(F32) + fin_y[...].astype(F32))
+
+    def line_sum_step(which, staged, from_u, from_d, k):
+        for way in range(2):
+            if way == 0:
+                j, on, more, buf, device = a - k, z < a - k, z > 0, from_u, above
+            else:
+                j, on, more, buf, device = k - 1, z > k - 1, z < a - 1, from_d, below
+
+            @pl.when(on & more)
+            def _(j=j, buf=buf, way=way):
+                arrive(buf.at[j], rl_ss.at[which, 0, 0], rl_rs.at[which, way, j])
+                staged[j] = (staged[j].astype(F32) + buf[j].astype(F32)).astype(BF16)
+
+            send(staged.at[j], buf.at[j], rl_ss.at[which, way, j], rl_rs.at[which, way, j], device, on)
+
+    def line_sum_end(which, own, from_u, from_d, out):
+        @pl.when(z > 0)
+        def _():
+            arrive(from_u.at[z], rl_ss.at[which, 0, 0], rl_rs.at[which, 0, z])
+            own[slot(z)] = own[slot(z)] + from_u[z].astype(F32)
+
+        @pl.when(z < a - 1)
+        def _():
+            arrive(from_d.at[z], rl_ss.at[which, 0, 0], rl_rs.at[which, 1, z])
+            own[slot(z)] = own[slot(z)] + from_d[z].astype(F32)
+
+        out[...] = own[slot(z)].astype(BF16)
+
+    def columns(block, unit):
+        return pl.ds(pl.multiple_of(block * unit, unit), unit)
+
+    square_send(1, down_w, down_g)
+    line_gather(0, cot, cot_g, 0)
+    for o in range(1, a):
+        zd = lax.rem(z + o, a)
+        for u in range(half_side):
+            b = t * half_side + u
+            send(early_pre.at[:, columns(zd * side + b, ff)], pre_g.at[b, slot(z)],
+                 e_ss.at[0, o, u], e_rs.at[0, o, u], (zd * side + q, t))
+    down_g[q] = down_w[...]
+    up_g[q] = up_w[...]
+    cot_g[slot(z)] = cot[...]
+    late_g[slot(z)] = late_in[...]
+    early_g[slot(z)] = early_in[...]
+    for b in range(side):
+        pre_g[b, slot(z)] = early_pre[:, columns(z * side + b, ff)]
+
+    line_gather(0, cot, cot_g, 1)
+    square_relay(1, down_g)
+    square_send(0, up_w, up_g)
+    line_gather(1, late_in, late_g, 0)
+    for d in range(2, a):
+        line_gather(0, cot, cot_g, d)
+    for o in range(1, a):
+        zs = lax.rem(z - o + a, a)
+        for u in range(half_side):
+            b = t * half_side + u
+            place = pre_g.at[b, slot(zs)]
+            arrive(place, e_ss.at[0, 0, 0], e_rs.at[0, o, u])
+            send(place, place, e_ss.at[1, o, u], e_rs.at[1, o, u], pn)
+    line_gather(1, late_in, late_g, 1)
+    line_gather(2, early_in, early_g, 0)
+    square_rest(1, down_g)
+
+    @pl.loop(0, side)
+    def _(b):
+        gt_s[b] = dot(cot_g[...], down_g[b], 1, 1).astype(BF16)
+
+    send(gt_s, gt_r, t_ss.at[0], t_rs.at[0], pn)
+    for d in range(2, a):
+        line_gather(1, late_in, late_g, d)
+    square_relay(0, up_g)
+    for o in range(1, a):
+        zs = lax.rem(z - o + a, a)
+        for u in range(half_side):
+            b = (1 - t) * half_side + u
+            arrive(pre_g.at[b, slot(zs)], e_ss.at[0, 0, 0], e_rs.at[1, o, u])
+
+    @pl.loop(0, side)
+    def _(b):
+        eh[b] = square_relu(pre_g[b])
+
+    square_sum_begin(1, lambda b: dot(eh[b], cot_g[...], 0, 0), dg_s, dg_x, dg_y, dg_fx, dg_fy)
+    down_o[...] = down_sum[...] + dot(eh[q], cot_g[...], 0, 0)
+    arrive(gt_r, t_ss.at[0], t_rs.at[0])
+
+    @pl.loop(0, side)
+    def _(b):
+        hidden = gt_s[b].astype(F32) + gt_r[b].astype(F32)
+        pg[b] = (hidden * 2.0 * jnp.maximum(pre_g[b].astype(F32), 0.0)).astype(BF16)
+
+    line_gather(2, early_in, early_g, 1)
+    square_rest(0, up_g)
+
+    @pl.loop(0, side)
+    def _(b):
+        lt_s[b] = dot(late_g[...], up_g[b], 1, 0).astype(BF16)
+
+    send(lt_s, lt_r, t_ss.at[1], t_rs.at[1], pn)
+
+    def to_line(which, value, staged):
+        @pl.loop(0, side)
+        def _(n):
+            at = columns(n, step_n)
+            part[which, :, at] = value(at)
+
+        for j in range(a):
+            staged[j] = part[which, pl.ds(j * rows, rows)].astype(BF16)
+
+    def ig_value(at):
+        return sum(dot(pg[b], up_g[b, at, :], 1, 1) for b in range(side))
+
+    to_line(0, ig_value, ig_s)
+    line_sum_step(0, ig_s, ig_u, ig_d, 1)
+    if a > 2:
+        line_gather(2, early_in, early_g, 2)
+    square_sum_relay(1, dg_s, dg_x, dg_y, dg_fx, dg_fy)
+    arrive(lt_r, t_ss.at[1], t_rs.at[1])
+
+    @pl.loop(0, side)
+    def _(b):
+        pre = (lt_s[b].astype(F32) + lt_r[b].astype(F32)).astype(BF16)
+        lp[b] = pre
+        lh[b] = square_relu(pre)
+
+    for o in range(1, a):
+        zd = lax.rem(z + o, a)
+        for u in range(half_side):
+            b = t * half_side + u
+            send(lp.at[b, slot(zd)], lp_g.at[:, columns(z * side + b, ff)],
+                 l_ss.at[0, o, u], l_rs.at[0, o, u], (zd * side + q, t))
+    for b in range(side):
+        lp_g[:, columns(z * side + b, ff)] = lp[b, slot(z)]
+
+    def lo_value(at):
+        return sum(dot(lh[b], down_g[b, :, at], 1, 0) for b in range(side))
+
+    to_line(1, lo_value, lo_s)
+    for k in range(2, a):
+        line_sum_step(0, ig_s, ig_u, ig_d, k)
+        if k == 2:
+            line_sum_step(1, lo_s, lo_u, lo_d, 1)
+    for d in range(3, a):
+        line_gather(2, early_in, early_g, d)
+    square_sum_begin(0, lambda b: dot(early_g[...], pg[b], 0, 0), ug_s, ug_x, ug_y, ug_fx, ug_fy)
+    for o in range(1, a):
+        zs = lax.rem(z - o + a, a)
+        for u in range(half_side):
+            place = lp_g.at[:, columns(zs * side + t * half_side + u, ff)]
+            arrive(place, l_ss.at[0, 0, 0], l_rs.at[0, o, u])
+            send(place, place, l_ss.at[1, o, u], l_rs.at[1, o, u], pn)
+    for k in range(2 if a > 2 else 1, a):
+        line_sum_step(1, lo_s, lo_u, lo_d, k)
+    up_o[...] = up_sum[...] + dot(early_g[...], pg[q], 0, 0)
+    square_sum_relay(0, ug_s, ug_x, ug_y, ug_fx, ug_fy)
+    square_sum_end(1, dg_fx, dg_fy, down_o)
+    line_sum_end(0, part.at[0], ig_u, ig_d, in_grad_o)
+    line_sum_end(1, part.at[1], lo_u, lo_d, late_out_o)
+    for o in range(1, a):
+        zs = lax.rem(z - o + a, a)
+        for u in range(half_side):
+            place = lp_g.at[:, columns(zs * side + (1 - t) * half_side + u, ff)]
+            arrive(place, l_ss.at[0, 0, 0], l_rs.at[1, o, u])
+    late_pre_o[...] = lp_g[...]
+    square_sum_end(0, ug_fx, ug_fy, up_o)
+
+    for cond, copy in sent:
+        if cond is None:
+            copy.wait_send()
+        else:
+            pl.when(cond)(copy.wait_send)
+
+
+def fused_body(late_input, up_weight, down_weight, early_input, early_pre, cotangent, up_sum, down_sum):
+    a = lax.axis_size("fs") // 4
+    side = 4
+    rows, width = late_input.shape
+    ff = up_weight.shape[1]
+    tokens, hidden = rows * a, ff * side
+    V = pltpu.VMEM
+    D = pltpu.SemaphoreType.DMA
+    token_block = V((tokens, width), BF16)
+    hidden_block = V((side, tokens, ff), BF16)
+    line_block = V((a, rows, width), BF16)
+    scratch = (
+        [token_block] * 3
+        + [hidden_block, V((side, width, ff), BF16), V((side, ff, width), BF16)]
+        + [hidden_block] * 8
+        + [V((rows, hidden * a), BF16), V((2, tokens, width), F32)]
+        + [line_block] * 6
+        + [V((side, ff, width), BF16)] + [V((ff // 2, width), BF16)] * 2 + [V((ff, width), BF16)] * 2
+        + [V((side, width, ff), BF16)] + [V((width // 2, ff), BF16)] * 2 + [V((width, ff), BF16)] * 2
+        + [D((3, 2, a)), D((3, 2, a)), D((2, 2, 3)), D((2, 2, 3)), D((2, a, 2)), D((2, a, 2)),
+           D((2, a, 2)), D((2, a, 2)), D((2,)), D((2,)), D((2, 2, a)), D((2, 2, a)), D((2, 6)), D((2, 6))]
+    )
+    flops = 12 * tokens * hidden * width
+    return pl.pallas_call(
+        lambda *refs: fused(a, *refs),
+        out_shape=(
+            jax.ShapeDtypeStruct(early_pre.shape, BF16),
+            jax.ShapeDtypeStruct(late_input.shape, BF16),
+            jax.ShapeDtypeStruct(early_input.shape, BF16),
+            jax.ShapeDtypeStruct(up_sum.shape, F32),
+            jax.ShapeDtypeStruct(down_sum.shape, F32),
+        ),
+        in_specs=[pl.BlockSpec(memory_space=pltpu.VMEM)] * 8,
+        out_specs=[pl.BlockSpec(memory_space=pltpu.VMEM)] * 5,
+        scratch_shapes=scratch,
+        compiler_params=pltpu.CompilerParams(
+            collective_id=0, has_side_effects=True, vmem_limit_bytes=62 * 1024 * 1024),
+        cost_estimate=pl.CostEstimate(flops=flops, bytes_accessed=1 << 24, transcendentals=0),
+    )(late_input, up_weight, down_weight, early_input, early_pre, cotangent, up_sum, down_sum)
 
 
 def contract_rows(left, right):
@@ -56,4 +410,6 @@
         P("fs", "tp"),
     )
     out_specs = (P("fs", None), P("fs", "tp"), P("fs", "tp"), P("tp", "fs"), P("fs", "tp"))
-    return jax.shard_map(body, mesh=mesh, in_specs=in_specs, out_specs=out_specs, check_vma=False)
+    square_chips = mesh.shape["tp"] == 2 and mesh.shape["fs"] % 4 == 0 and mesh.shape["fs"] >= 8
+    chosen = fused_body if square_chips else body
+    return jax.shard_map(chosen, mesh=mesh, in_specs=in_specs, out_specs=out_specs, check_vma=False)

time: 476 us -> 133 us (0.28)
  waiting for transfers between devices: 406 us -> 0 us
  Pallas kernels: 0 us -> 126 us
  matrix products: 34.3 us -> 0 us
  between operations: 13.8 us -> 0.66 us
  starting transfers between devices: 12.3 us -> 0 us
    all_gather x4 -> x0, waiting for transfers between devices: 351 us -> none  [the longest x1 126 us: body(): up_gathered = lax.all_gather(up_weight, 'fs', axis=1, tiled=True)]
    pallas_call x0 -> x1, Pallas kernels: none -> 126 us  [fused_body(): pl.pallas_call(lambda *refs: fused(a, *refs), out_shape=(jax.ShapeDtypeSt...]
    dot_general x6 -> x0, matrix products: 34.3 us -> none  [the longest x2 14.4 us: contract_cols(): lax.dot_general(left, right, (((1,), (1,)), ((), ())), preferred_element_...]
    all_to_all x2 -> x0, waiting for transfers between devices: 30.6 us -> none  [the longest x1 30.6 us: body(): lax.all_to_all(pre_grad, 'fs', split_axis=1, concat_axis=0, tiled=True)]
    psum x1 -> x0, waiting for transfers between devices: 21.8 us -> none  [body(): pre_summed = lax.psum(pre_terms.astype(jnp.bfloat16), 'tp')]
    all_to_all x2 -> x0, starting transfers between devices: 12.2 us -> none  [the longest x1 6.97 us: body(): lax.all_to_all(pre_grad, 'fs', split_axis=1, concat_axis=0, tiled=True)]
  transfers between devices with their start and end apart: 7 -> 0, of which waited for: 6 -> 0; matrix products, arithmetic and copies ran while one was open for 6% -> 0% of each run, Pallas kernels for 0% -> 0%
where the time goes in v1:
time: 133 us
  Pallas kernels  126 us (95%)
  local copies, waits for them, and re-layouts  6.71 us (5%)
    pallas_call x1, Pallas kernels, fused_body(): pl.pallas_call(lambda *refs: fused(a, *refs), out_shape=(jax.ShapeDtypeSt...  126 us
    unnamed x13, local copies, waits for them, and re-layouts  6.71 us

profile of v1, /device:TPU:8, one launch (start us, length us, event | category | flops | bytes accessed | tf_op | source)
XLA Modules:
  0.0 133.0 jit_solution(1894918856829298726)
XLA Ops:
  0.6 125.6 %shard_map.119 = (bf16[128,4096]{1,0:T(8,128)(2,1)}, bf16[128,1024]{1,0:T(8,128)(2,1)}, bf16[128,1024]{1,0:T(8,128)(2,1)}, f32[1024,256]{1,0:T(8,128)}, f32[256,1024]{1,0:T(8,128)}) custom-call(bf16[128,1024]{1,0:T(8,128)(2,1)} %refs_0_.1, bf16[1024,256]{1,0:T(8,128)(2,1)} %refs_1_.1, bf16[256,1024]{1,0:T(8,128)(2,1)} %refs_2_.1, bf16[128,1024]{1,0:T(8,128)(2,1)} %refs_3_.1, ...), custom_call_target="tpu_custom_call" | custom-call | flops 6442450944 | bytes 16777216 | tf_op jit(solution)/shard_map/pallas_call | solution.py:343
  126.2 0.0 copy-start.3
  126.3 0.0 copy-start.1
  126.3 2.4 %copy.18 = bf16[128,4096]{1,0:T(8,128)(2,1)} copy(bf16[128,4096]{1,0:T(8,128)(2,1)} %get-tuple-element.10) | data formatting | bytes 2097152
  128.7 0.0 copy-done.3
  128.7 0.0 copy-start.2
  128.7 0.7 copy.19
  129.4 0.3 copy-done.2
  129.7 0.7 copy.20
  130.4 0.0 copy-done.1
  130.4 0.0 copy-start
  130.4 1.0 copy.21
  131.4 0.6 copy-done
  132.0 1.0 copy.22
Async XLA Ops:
  126.2 2.4 %copy-start.3 = (bf16[128,1024]{1,0:T(8,128)(2,1)S(1)}, bf16[128,1024]{1,0:T(8,128)(2,1)}, u32[]{:S(2)}) copy-start(bf16[128,1024]{1,0:T(8,128)(2,1)} %get-tuple-element.11) | copy-start | bytes 786436
  126.3 4.2 %copy-start.1 = (f32[1024,256]{1,0:T(8,128)S(1)}, f32[1024,256]{1,0:T(8,128)}, u32[]{:S(2)}) copy-start(f32[1024,256]{1,0:T(8,128)} %get-tuple-element.13) | copy-start | bytes 3145732
  128.7 1.0 copy-start.2
  130.4 1.6 %copy-start = (f32[256,1024]{1,0:T(8,128)S(1)}, f32[256,1024]{1,0:T(8,128)}, u32[]{:S(2)}) copy-start(f32[256,1024]{1,0:T(8,128)} %get-tuple-element.14) | copy-start | bytes 3145732

commit v2 on v1

--- a/solution.py
+++ b/solution.py
@@ -19,12 +19,13 @@
     return (kept * kept).astype(BF16)
 
 
-def fused(a, late_in, up_w, down_w, early_in, early_pre, cot, up_sum, down_sum,
+def fused(a, late_in, up_w, down_w, early_in, early_pre, cot,
           late_pre_o, late_out_o, in_grad_o, up_o, down_o,
           cot_g, late_g, early_g, pre_g, up_g, down_g, gt_s, gt_r, pg, eh, lt_s, lt_r, lp, lh, lp_g,
           part, ig_s, ig_u, ig_d, lo_s, lo_u, lo_d,
           dg_s, dg_x, dg_y, dg_fx, dg_fy, ug_s, ug_x, ug_y, ug_fx, ug_fy,
-          ag_ss, ag_rs, w_ss, w_rs, e_ss, e_rs, l_ss, l_rs, t_ss, t_rs, rl_ss, rl_rs, rq_ss, rq_rs):
+          ag_ss, ag_rs, w_ss, w_rs, e_ss, e_rs, l_ss, l_rs, t_ss, t_rs, rl_ss, rl_rs, rq_ss, rq_rs,
+          local_s, down_v, up_v, ig_v, lo_v):
     side = 4
     half_side = side // 2
     me = lax.axis_index("fs")
@@ -47,6 +48,23 @@
     cols = ff * side
     step_n = width // side
 
+    def begin(src, dst, k):
+        copy = pltpu.make_async_copy(src, dst, local_s.at[k])
+        copy.start()
+        return copy
+
+    own_rows = pl.ds(pl.multiple_of(z * rows, rows), rows)
+    own_down = begin(down_w, down_g.at[q], 0)
+    own_cot = begin(cot, cot_g.at[own_rows], 1)
+    own_up = begin(up_w, up_g.at[q], 2)
+    own_late = begin(late_in, late_g.at[own_rows], 3)
+    own_early = begin(early_in, early_g.at[own_rows], 4)
+    own_pre = [
+        begin(early_pre.at[:, pl.ds(pl.multiple_of((z * side + b) * ff, ff), ff)],
+              pre_g.at[b, own_rows], 5 + b)
+        for b in range(side)
+    ]
+
     barrier = pltpu.get_barrier_semaphore()
     greet = [xn, yn, pn] + [(lax.rem(me + o * side, a * side), t) for o in range(1, a)]
     for device in greet:
@@ -145,19 +163,20 @@
         arrive(half2(fin_x, 1), rq_ss.at[which, 0], rq_rs.at[which, 5])
         out[...] = out[...] + (fin_x[...].astype(F32) + fin_y[...].astype(F32))
 
-    def line_sum_step(which, staged, from_u, from_d, k):
+    def line_sum_step(which, staged, from_u, from_d, step):
         for way in range(2):
             if way == 0:
-                j, on, more, buf, device = a - k, z < a - k, z > 0, from_u, above
+                j, on, more, buf, device = a - 1 + z - step, step >= z, z > 0, from_u, above
             else:
-                j, on, more, buf, device = k - 1, z > k - 1, z < a - 1, from_d, below
+                j, on, more, buf, device = step - (a - 1 - z), step >= a - 1 - z, z < a - 1, from_d, below
+            j = jnp.clip(j, 0, a - 1)
 
             @pl.when(on & more)
             def _(j=j, buf=buf, way=way):
                 arrive(buf.at[j], rl_ss.at[which, 0, 0], rl_rs.at[which, way, j])
                 staged[j] = (staged[j].astype(F32) + buf[j].astype(F32)).astype(BF16)
 
-            send(staged.at[j], buf.at[j], rl_ss.at[which, way, j], rl_rs.at[which, way, j], device, on)
+            send(staged.at[j], buf.at[j], rl_ss.at[which, way, step], rl_rs.at[which, way, j], device, on)
 
     def line_sum_end(which, own, from_u, from_d, out):
         @pl.when(z > 0)
@@ -175,74 +194,14 @@
     def columns(block, unit):
         return pl.ds(pl.multiple_of(block * unit, unit), unit)
 
-    square_send(1, down_w, down_g)
-    line_gather(0, cot, cot_g, 0)
-    for o in range(1, a):
-        zd = lax.rem(z + o, a)
-        for u in range(half_side):
-            b = t * half_side + u
-            send(early_pre.at[:, columns(zd * side + b, ff)], pre_g.at[b, slot(z)],
-                 e_ss.at[0, o, u], e_rs.at[0, o, u], (zd * side + q, t))
-    down_g[q] = down_w[...]
-    up_g[q] = up_w[...]
-    cot_g[slot(z)] = cot[...]
-    late_g[slot(z)] = late_in[...]
-    early_g[slot(z)] = early_in[...]
-    for b in range(side):
-        pre_g[b, slot(z)] = early_pre[:, columns(z * side + b, ff)]
-
-    line_gather(0, cot, cot_g, 1)
-    square_relay(1, down_g)
-    square_send(0, up_w, up_g)
-    line_gather(1, late_in, late_g, 0)
-    for d in range(2, a):
-        line_gather(0, cot, cot_g, d)
-    for o in range(1, a):
-        zs = lax.rem(z - o + a, a)
-        for u in range(half_side):
-            b = t * half_side + u
-            place = pre_g.at[b, slot(zs)]
-            arrive(place, e_ss.at[0, 0, 0], e_rs.at[0, o, u])
-            send(place, place, e_ss.at[1, o, u], e_rs.at[1, o, u], pn)
-    line_gather(1, late_in, late_g, 1)
-    line_gather(2, early_in, early_g, 0)
-    square_rest(1, down_g)
-
-    @pl.loop(0, side)
-    def _(b):
-        gt_s[b] = dot(cot_g[...], down_g[b], 1, 1).astype(BF16)
-
-    send(gt_s, gt_r, t_ss.at[0], t_rs.at[0], pn)
-    for d in range(2, a):
-        line_gather(1, late_in, late_g, d)
-    square_relay(0, up_g)
-    for o in range(1, a):
-        zs = lax.rem(z - o + a, a)
-        for u in range(half_side):
-            b = (1 - t) * half_side + u
-            arrive(pre_g.at[b, slot(zs)], e_ss.at[0, 0, 0], e_rs.at[1, o, u])
-
-    @pl.loop(0, side)
-    def _(b):
-        eh[b] = square_relu(pre_g[b])
-
-    square_sum_begin(1, lambda b: dot(eh[b], cot_g[...], 0, 0), dg_s, dg_x, dg_y, dg_fx, dg_fy)
-    down_o[...] = down_sum[...] + dot(eh[q], cot_g[...], 0, 0)
-    arrive(gt_r, t_ss.at[0], t_rs.at[0])
-
-    @pl.loop(0, side)
-    def _(b):
-        hidden = gt_s[b].astype(F32) + gt_r[b].astype(F32)
-        pg[b] = (hidden * 2.0 * jnp.maximum(pre_g[b].astype(F32), 0.0)).astype(BF16)
-
-    line_gather(2, early_in, early_g, 1)
-    square_rest(0, up_g)
-
-    @pl.loop(0, side)
-    def _(b):
-        lt_s[b] = dot(late_g[...], up_g[b], 1, 0).astype(BF16)
-
-    send(lt_s, lt_r, t_ss.at[1], t_rs.at[1], pn)
+    def hops(b_of, go):
+        for o in range(1, a):
+            zs = lax.rem(z - o + a, a)
+            for u in range(half_side):
+                go(o, u, zs, b_of(u))
+
+    mine = lambda u: t * half_side + u
+    other = lambda u: (1 - t) * half_side + u
 
     def to_line(which, value, staged):
         @pl.loop(0, side)
@@ -253,13 +212,107 @@
         for j in range(a):
             staged[j] = part[which, pl.ds(j * rows, rows)].astype(BF16)
 
+    def pre_relay(o, u, zs, b):
+        place = pre_g.at[b, slot(zs)]
+        arrive(place, e_ss.at[0, 0, 0], e_rs.at[0, o, u])
+        send(place, place, e_ss.at[1, o, u], e_rs.at[1, o, u], pn)
+
+    def pre_rest(o, u, zs, b):
+        arrive(pre_g.at[b, slot(zs)], e_ss.at[0, 0, 0], e_rs.at[1, o, u])
+
+    def out_relay(o, u, zs, b):
+        place = lp_g.at[:, columns(zs * side + b, ff)]
+        arrive(place, l_ss.at[0, 0, 0], l_rs.at[0, o, u])
+        send(place, place, l_ss.at[1, o, u], l_rs.at[1, o, u], pn)
+
+    def out_rest(o, u, zs, b):
+        arrive(lp_g.at[:, columns(zs * side + b, ff)], l_ss.at[0, 0, 0], l_rs.at[1, o, u])
+
+    def gather_late(d):
+        if d < a:
+            line_gather(1, late_g.at[slot(z)], late_g, d)
+
+    def gather_early(d):
+        if d < a:
+            line_gather(2, early_g.at[slot(z)], early_g, d)
+
+    def gather_cot(d):
+        if d < a:
+            line_gather(0, cot_g.at[slot(z)], cot_g, d)
+
+    def sum_ig(k):
+        if k < a:
+            line_sum_step(0, ig_s, ig_u, ig_d, k - 1)
+
+    def sum_lo(k):
+        if k < a:
+            line_sum_step(1, lo_s, lo_u, lo_d, k - 1)
+
+    own_down.wait()
+    square_send(1, down_g.at[q], down_g)
+    own_cot.wait()
+    gather_cot(0)
+    for o in range(1, a):
+        zd = lax.rem(z + o, a)
+        for u in range(half_side):
+            b = mine(u)
+            send(early_pre.at[:, columns(zd * side + b, ff)], pre_g.at[b, slot(z)],
+                 e_ss.at[0, o, u], e_rs.at[0, o, u], (zd * side + q, t))
+    for copy in own_pre:
+        copy.wait()
+    gather_cot(1)
+    square_relay(1, down_g)
+    own_up.wait()
+    square_send(0, up_g.at[q], up_g)
+    own_late.wait()
+    gather_late(0)
+    gather_cot(2)
+    hops(mine, pre_relay)
+    for d in range(3, a):
+        gather_cot(d)
+    square_rest(1, down_g)
+    gather_late(1)
+    square_relay(0, up_g)
+
+    @pl.loop(0, side)
+    def _(b):
+        gt_s[b] = dot(cot_g[...], down_g[b], 1, 1).astype(BF16)
+
+    send(gt_s, gt_r, t_ss.at[0], t_rs.at[0], pn)
+    own_early.wait()
+    gather_early(0)
+    hops(other, pre_rest)
+
+    @pl.loop(0, side)
+    def _(b):
+        eh[b] = square_relu(pre_g[b])
+
+    square_sum_begin(1, lambda b: dot(eh[b], cot_g[...], 0, 0), dg_s, dg_x, dg_y, dg_fx, dg_fy)
+    arrive(gt_r, t_ss.at[0], t_rs.at[0])
+
+    @pl.loop(0, side)
+    def _(b):
+        hidden = gt_s[b].astype(F32) + gt_r[b].astype(F32)
+        pg[b] = (hidden * 2.0 * jnp.maximum(pre_g[b].astype(F32), 0.0)).astype(BF16)
+
+    gather_late(2)
+    square_rest(0, up_g)
+
     def ig_value(at):
         return sum(dot(pg[b], up_g[b, at, :], 1, 1) for b in range(side))
 
     to_line(0, ig_value, ig_s)
-    line_sum_step(0, ig_s, ig_u, ig_d, 1)
-    if a > 2:
-        line_gather(2, early_in, early_g, 2)
+    sum_ig(1)
+    for d in range(3, a):
+        gather_late(d)
+
+    @pl.loop(0, side)
+    def _(b):
+        lt_s[b] = dot(late_g[...], up_g[b], 1, 0).astype(BF16)
+
+    send(lt_s, lt_r, t_ss.at[1], t_rs.at[1], pn)
+    sum_ig(2)
+    gather_early(1)
     square_sum_relay(1, dg_s, dg_x, dg_y, dg_fx, dg_fy)
     arrive(lt_r, t_ss.at[1], t_rs.at[1])
 
@@ -272,7 +325,7 @@
     for o in range(1, a):
         zd = lax.rem(z + o, a)
         for u in range(half_side):
-            b = t * half_side + u
+            b = mine(u)
             send(lp.at[b, slot(zd)], lp_g.at[:, columns(z * side + b, ff)],
                  l_ss.at[0, o, u], l_rs.at[0, o, u], (zd * side + q, t))
     for b in range(side):
@@ -282,39 +335,38 @@
         return sum(dot(lh[b], down_g[b, :, at], 1, 0) for b in range(side))
 
     to_line(1, lo_value, lo_s)
-    for k in range(2, a):
-        line_sum_step(0, ig_s, ig_u, ig_d, k)
-        if k == 2:
-            line_sum_step(1, lo_s, lo_u, lo_d, 1)
+    sum_lo(1)
+    gather_early(2)
+    for k in range(3, a):
+        sum_ig(k)
+    sum_lo(2)
+    down_v[...] = dot(eh[q], cot_g[...], 0, 0)
     for d in range(3, a):
-        line_gather(2, early_in, early_g, d)
+        gather_early(d)
     square_sum_begin(0, lambda b: dot(early_g[...], pg[b], 0, 0), ug_s, ug_x, ug_y, ug_fx, ug_fy)
-    for o in range(1, a):
-        zs = lax.rem(z - o + a, a)
-        for u in range(half_side):
-            place = lp_g.at[:, columns(zs * side + t * half_side + u, ff)]
-            arrive(place, l_ss.at[0, 0, 0], l_rs.at[0, o, u])
-            send(place, place, l_ss.at[1, o, u], l_rs.at[1, o, u], pn)
-    for k in range(2 if a > 2 else 1, a):
-        line_sum_step(1, lo_s, lo_u, lo_d, k)
-    up_o[...] = up_sum[...] + dot(early_g[...], pg[q], 0, 0)
+    up_v[...] = dot(early_g[...], pg[q], 0, 0)
+    hops(mine, out_relay)
+    square_sum_end(1, dg_fx, dg_fy, down_v)
+    out_down = begin(down_v, down_o, 9)
+    for k in range(3, a):
+        sum_lo(k)
+    line_sum_end(0, part.at[0], ig_u, ig_d, ig_v)
+    out_ig = begin(ig_v, in_grad_o, 10)
     square_sum_relay(0, ug_s, ug_x, ug_y, ug_fx, ug_fy)
-    square_sum_end(1, dg_fx, dg_fy, down_o)
-    line_sum_end(0, part.at[0], ig_u, ig_d, in_grad_o)
-    line_sum_end(1, part.at[1], lo_u, lo_d, late_out_o)
-    for o in range(1, a):
-        zs = lax.rem(z - o + a, a)
-        for u in range(half_side):
-            place = lp_g.at[:, columns(zs * side + (1 - t) * half_side + u, ff)]
-            arrive(place, l_ss.at[0, 0, 0], l_rs.at[1, o, u])
-    late_pre_o[...] = lp_g[...]
-    square_sum_end(0, ug_fx, ug_fy, up_o)
+    hops(other, out_rest)
+    out_pre = begin(lp_g, late_pre_o, 11)
+    line_sum_end(1, part.at[1], lo_u, lo_d, lo_v)
+    out_lo = begin(lo_v, late_out_o, 12)
+    square_sum_end(0, ug_fx, ug_fy, up_v)
+    out_up = begin(up_v, up_o, 13)
 
     for cond, copy in sent:
         if cond is None:
             copy.wait_send()
         else:
             pl.when(cond)(copy.wait_send)
+    for copy in (out_down, out_ig, out_pre, out_lo, out_up):
+        copy.wait()
 
 
 def fused_body(late_input, up_weight, down_weight, early_input, early_pre, cotangent, up_sum, down_sum):
@@ -337,10 +389,11 @@
         + [V((side, ff, width), BF16)] + [V((ff // 2, width), BF16)] * 2 + [V((ff, width), BF16)] * 2
         + [V((side, width, ff), BF16)] + [V((width // 2, ff), BF16)] * 2 + [V((width, ff), BF16)] * 2
         + [D((3, 2, a)), D((3, 2, a)), D((2, 2, 3)), D((2, 2, 3)), D((2, a, 2)), D((2, a, 2)),
-           D((2, a, 2)), D((2, a, 2)), D((2,)), D((2,)), D((2, 2, a)), D((2, 2, a)), D((2, 6)), D((2, 6))]
+           D((2, a, 2)), D((2, a, 2)), D((2,)), D((2,)), D((2, 2, a)), D((2, 2, a)), D((2, 6)), D((2, 6)), D((14,))]
+        + [V((ff, width), F32), V((width, ff), F32)] + [V((rows, width), BF16)] * 2
     )
     flops = 12 * tokens * hidden * width
-    return pl.pallas_call(
+    late_pre, late_out, input_grad, up_grad, down_grad = pl.pallas_call(
         lambda *refs: fused(a, *refs),
         out_shape=(
             jax.ShapeDtypeStruct(early_pre.shape, BF16),
@@ -349,13 +402,14 @@
             jax.ShapeDtypeStruct(up_sum.shape, F32),
             jax.ShapeDtypeStruct(down_sum.shape, F32),
         ),
-        in_specs=[pl.BlockSpec(memory_space=pltpu.VMEM)] * 8,
-        out_specs=[pl.BlockSpec(memory_space=pltpu.VMEM)] * 5,
+        in_specs=[pl.BlockSpec(memory_space=pl.ANY)] * 6,
+        out_specs=[pl.BlockSpec(memory_space=pl.ANY)] * 5,
         scratch_shapes=scratch,
         compiler_params=pltpu.CompilerParams(
             collective_id=0, has_side_effects=True, vmem_limit_bytes=62 * 1024 * 1024),
         cost_estimate=pl.CostEstimate(flops=flops, bytes_accessed=1 << 24, transcendentals=0),
-    )(late_input, up_weight, down_weight, early_input, early_pre, cotangent, up_sum, down_sum)
+    )(late_input, up_weight, down_weight, early_input, early_pre, cotangent)
+    return late_pre, late_out, input_grad, up_sum + up_grad, down_sum + down_grad
 
 
 def contract_rows(left, right):

time: 133 us -> 106 us (0.80)
  Pallas kernels: 126 us -> 97.5 us
  other arithmetic: 0 us -> 3.58 us
  local copies, waits for them, and re-layouts: 6.71 us -> 3.35 us
    pallas_call x1, Pallas kernels: 126 us -> 97.5 us  [fused_body(): pl.pallas_call(lambda *refs: fused(a, *refs), out_shape=(jax.ShapeDtypeSt...]
    add x0 -> x2, other arithmetic: none -> 3.58 us  [the longest x1 2.48 us: fused_body(): up_sum + up_grad]
    unnamed x13 -> x15, local copies, waits for them, and re-layouts: 6.71 us -> 3.35 us
where the time goes in v2:
time: 106 us; the launch traced here: 105 us
  Pallas kernels  97.5 us (92%)
  other arithmetic  3.58 us (3%)
  local copies, waits for them, and re-layouts  3.35 us (3%)
    pallas_call x1, Pallas kernels, fused_body(): pl.pallas_call(lambda *refs: fused(a, *refs), out_shape=(jax.ShapeDtypeSt...  97.5 us
    unnamed x15, local copies, waits for them, and re-layouts  3.35 us
    add x1, other arithmetic, fused_body(): up_sum + up_grad  2.48 us

profile of v2, /device:TPU:8, one launch (start us, length us, event | category | flops | bytes accessed | tf_op | source)
XLA Modules:
  0.0 105.1 jit_solution(10523230525857273821)
XLA Ops:
  0.6 0.0 copy-start
  0.6 97.5 %shard_map.119 = (bf16[128,4096]{1,0:T(8,128)(2,1)}, bf16[128,1024]{1,0:T(8,128)(2,1)}, bf16[128,1024]{1,0:T(8,128)(2,1)}, f32[1024,256]{1,0:T(8,128)}, f32[256,1024]{1,0:T(8,128)}) custom-call(bf16[128,1024]{1,0:T(8,128)(2,1)} %refs_0_.1, bf16[1024,256]{1,0:T(8,128)(2,1)} %refs_1_.1, bf16[256,1024]{1,0:T(8,128)(2,1)} %refs_2_.1, bf16[128,1024]{1,0:T(8,128)(2,1)} %refs_3_.1, ...), custom_call_target="tpu_custom_call" | custom-call | flops 6442450944 | bytes 16777216 | tf_op jit(solution)/shard_map/pallas_call | solution.py:396
  98.2 0.0 copy-done
  98.2 0.0 copy-start.1
  98.2 0.0 copy-start.2
  98.2 2.5 %add.6 = f32[1024,256]{1,0:T(8,128)} add(f32[1024,256]{1,0:T(8,128)S(1)} %copy-done, f32[1024,256]{1,0:T(8,128)} %get-tuple-element.13) | non-fusion elementwise | flops 262144 | bytes 3145728 | tf_op jit(solution)/shard_map/add | solution.py:412
  100.7 0.0 copy-done.1
  100.7 0.0 copy-done.2
  100.7 0.0 copy-start.3
  100.7 1.1 %add.7 = f32[256,1024]{1,0:T(8,128)} add(f32[256,1024]{1,0:T(8,128)S(1)} %copy-done.1, f32[256,1024]{1,0:T(8,128)S(1)} %copy-done.2) | non-fusion elementwise | flops 262144 | bytes 3145728 | tf_op jit(solution)/shard_map/add | solution.py:412
  101.8 0.5 copy-done.3
  102.3 0.0 copy-start.5
  102.3 1.0 copy.16
  103.3 0.1 copy-done.5
  103.4 0.0 copy-start.4
  103.4 0.7 copy.17
  104.1 0.3 copy-done.4
  104.4 0.7 copy.18
Async XLA Ops:
  0.6 97.5 %copy-start = (f32[1024,256]{1,0:T(8,128)S(1)}, f32[1024,256]{1,0:T(8,128)}, u32[]{:S(2)}) copy-start(f32[1024,256]{1,0:T(8,128)} %param.14) | copy-start | bytes 3145732
  98.2 2.5 %copy-start.1 = (f32[256,1024]{1,0:T(8,128)S(1)}, f32[256,1024]{1,0:T(8,128)}, u32[]{:S(2)}) copy-start(f32[256,1024]{1,0:T(8,128)} %param.15) | copy-start | bytes 3145732
  98.2 2.5 %copy-start.2 = (f32[256,1024]{1,0:T(8,128)S(1)}, f32[256,1024]{1,0:T(8,128)}, u32[]{:S(2)}) copy-start(f32[256,1024]{1,0:T(8,128)} %get-tuple-element.14) | copy-start | bytes 3145732
  100.7 1.6 %copy-start.3 = (bf16[128,4096]{1,0:T(8,128)(2,1)S(1)}, bf16[128,4096]{1,0:T(8,128)(2,1)}, u32[]{:S(2)}) copy-start(bf16[128,4096]{1,0:T(8,128)(2,1)} %get-tuple-element.20) | copy-start | bytes 3145732
  102.3 1.1 %copy-start.5 = (bf16[128,1024]{1,0:T(8,128)(2,1)S(1)}, bf16[128,1024]{1,0:T(8,128)(2,1)}, u32[]{:S(2)}) copy-start(bf16[128,1024]{1,0:T(8,128)(2,1)} %get-tuple-element.21) | copy-start | bytes 786436
  103.4 1.0 copy-start.4
